TPU v7x, 32 devices: a whole 2x2x4 slice. The times are simulated.
32 devices in a mesh: sp: 16 (over z, y, x), tp: 2 (over core).
Axes of the slice: x: 2, y: 2, z: 4, core: 2. Of those that a mesh axis runs over, the one named last changes fastest.
Arguments:
- tokens: bfloat16 [4096, 2048], P('sp', 'tp'), may hold values from -6 to 6
- outer_gate: bfloat16 [2048, 1024], P(None, 'tp'), may hold values from -0.125 to 0.125
- inner_gate: bfloat16 [2048, 1024], P(None, 'tp'), may hold values from -0.125 to 0.125
- conv_input: bfloat16 [2048, 1024], P(None, 'tp'), may hold values from -0.125 to 0.125
- conv_taps: bfloat16 [3, 1024], P(None, 'tp'), may hold values from -3.5 to 3.5
- query_down: bfloat16 [2048, 512], P(None, 'tp'), may hold values from -0.125 to 0.125
- latent_down: bfloat16 [2048, 256], P(None, 'tp'), may hold values from -0.125 to 0.125
- rotary_down: bfloat16 [2048, 32], replicated, may hold values from -5.303301 to 5.303301
- query_gain: float32 [512], replicated, may hold values from 0.1 to 1.9
- latent_gain: float32 [256], replicated, may hold values from 0.1 to 1.9
- query_up: bfloat16 [512, 1536], P(None, 'tp'), may hold values from -0.52734375 to 0.52734375
- latent_up: bfloat16 [256, 2048], P(None, 'tp'), may hold values from -0.75 to 0.75
- conv_project: bfloat16 [1024, 2048], P('tp'), may hold values from -0.1875 to 0.1875
- attend_project: bfloat16 [1024, 2048], P('tp'), may hold values from -0.1875 to 0.1875
Outputs:
- mixed: bfloat16 [4096, 2048], P(('sp', 'tp'))
All inputs are finite; a program needn't handle non-finite values.
Results may differ from a plain program's by a relative error of at most 0.035.
Values may be sent and summed in bfloat16 or wider, within the bound.
A program may use at most 128 MiB of HBM per device.

v0:
```python
import math
import jax
import jax.numpy as jnp
from jax import lax
from jax.sharding import PartitionSpec as P

NOPE = 64
ROPE = 32
VDIM = 64
neg_fill = -1e30
rotary_base = 10000.0
norm_epsilon = 1e-06


def shifted(shard, axis, by):
    length = lax.axis_size(axis)
    pairs = [(i, i + by) for i in range(length) if 0 <= i + by < length]
    return lax.ppermute(shard, axis, pairs)


def rotate(values, positions):
    half = values.shape[-1] // 2
    inverse = rotary_base ** (-(jnp.arange(half, dtype=jnp.float32) * 2.0 / (2 * half)))
    angle = positions[:, None] * inverse[None, :]
    if values.ndim == 3:
        angle = angle[:, None, :]
    cosine = jnp.cos(angle)
    sine = jnp.sin(angle)
    first = values[..., :half]
    second = values[..., half:]
    return jnp.concatenate([first * cosine - second * sine, first * sine + second * cosine], -1)


def rms_scale(latent, gain):
    values = latent.astype(jnp.float32)
    factor = lax.rsqrt(jnp.mean(values * values, -1, keepdims=True) + norm_epsilon)
    return (values * factor * gain).astype(jnp.bfloat16)


def local(
    tokens,
    outer_gate,
    inner_gate,
    conv_input,
    conv_taps,
    query_down,
    latent_down,
    rotary_down,
    query_gain,
    latent_gain,
    query_up,
    latent_up,
    conv_project,
    attend_project,
):
    tok_rows = tokens.shape[0]
    local_heads = query_up.shape[1] // (NOPE + ROPE)
    weights = (outer_gate, inner_gate, conv_input, query_down, latent_down, rotary_down)
    piece = lax.all_gather(tokens, "tp", axis=1, tiled=True)
    outer, inner, signal, query_part, latent_part, rotary_raw = tuple(
        (jnp.dot(piece, weight, preferred_element_type=jnp.float32) for weight in weights)
    )
    query_lat, latent_lat = (
        lax.all_gather(query_part.astype(jnp.bfloat16), "tp", axis=1, tiled=True),
        lax.all_gather(latent_part.astype(jnp.bfloat16), "tp", axis=1, tiled=True),
    )
    gated = (inner * signal).astype(jnp.bfloat16)
    reach = conv_taps.shape[0] - 1
    rim = shifted(gated[tok_rows - reach :], "sp", 1)
    padded = jnp.concatenate([rim, gated], 0).astype(jnp.float32)
    taps = conv_taps.astype(jnp.float32)
    filtered = padded[0:tok_rows] * taps[0]
    for index in range(1, reach + 1):
        filtered = filtered + padded[index : index + tok_rows] * taps[index]
    conv_result = (outer * filtered).astype(jnp.bfloat16)
    seq_index = lax.axis_index("sp")
    offset = seq_index * tok_rows
    query_index = offset + jnp.arange(tok_rows, dtype=jnp.int32)
    positions = query_index.astype(jnp.float32)
    query_norm = rms_scale(query_lat, query_gain)
    latent_norm = rms_scale(latent_lat, latent_gain)
    rotary_key = rotate(rotary_raw, positions).astype(jnp.bfloat16)
    query_full = jnp.dot(query_norm, query_up, preferred_element_type=jnp.float32)
    query_full = query_full.reshape(tok_rows, local_heads, NOPE + ROPE)
    query_plain = query_full[..., :NOPE].astype(jnp.bfloat16)
    query_rot = rotate(query_full[..., NOPE:], positions).astype(jnp.bfloat16)
    scale = (NOPE + ROPE) ** (-0.5)
    query_sets = ((query_plain, query_rot, query_index),)
    set_lasts = tuple((jnp.max(members[2]) for members in query_sets))
    overall_last = set_lasts[0]

    def update(current, members, key_plain, values, rot_block, first, block):
        plain, turned, indices = members
        best, total, accum = current
        scores = jnp.einsum("qhd,khd->hqk", plain, key_plain, preferred_element_type=jnp.float32)
        scores = scores + jnp.einsum(
            "qhr,kr->hqk", turned, rot_block, preferred_element_type=jnp.float32
        )
        scores = scores * scale
        key_index = first + jnp.arange(block, dtype=jnp.int32)
        visible = key_index[None, :] <= indices[:, None]
        scores = jnp.where(visible[None], scores, neg_fill)
        new_best = jnp.maximum(best, jnp.max(scores, -1))
        factor = jnp.exp(best - new_best)
        weight = jnp.exp(scores - new_best[..., None])
        total = total * factor + jnp.sum(weight, -1)
        accum = accum * factor[..., None] + jnp.einsum(
            "hqk,khd->hqd", weight.astype(jnp.bfloat16), values, preferred_element_type=jnp.float32
        )
        return (new_best, total, accum)

    initial = tuple(
        (
            (
                jnp.full((local_heads, members[2].shape[0]), neg_fill, jnp.float32),
                jnp.zeros((local_heads, members[2].shape[0]), jnp.float32),
                jnp.zeros((local_heads, members[2].shape[0], VDIM), jnp.float32),
            )
            for members in query_sets
        )
    )
    carry = initial
    keys_latent = lax.all_gather(latent_norm, "sp", axis=0, tiled=True)
    keys_rot = lax.all_gather(rotary_key, "sp", axis=0, tiled=True)
    count = keys_latent.shape[0]
    block = math.gcd(count, 512)
    latent_blocks = keys_latent.reshape(count // block, block, keys_latent.shape[1])
    rot_blocks = keys_rot.reshape(count // block, block, keys_rot.shape[1])

    def advance(states, inputs):
        latent_block, rot_block, number = inputs
        first = number * block

        def compute(current):
            expanded = jnp.dot(latent_block, latent_up, preferred_element_type=jnp.float32)
            expanded = expanded.astype(jnp.bfloat16).reshape(block, local_heads, NOPE + VDIM)
            key_plain = expanded[..., :NOPE]
            values = expanded[..., NOPE:]
            results = []
            for members, last, state in zip(query_sets, set_lasts, current):
                results.append(
                    lax.cond(
                        first > last,
                        lambda kept: kept,
                        lambda kept, members=members: update(
                            kept, members, key_plain, values, rot_block, first, block
                        ),
                        state,
                    )
                )
            return tuple(results)

        return (lax.cond(first > overall_last, lambda current: current, compute, states), None)

    numbers = jnp.arange(count // block, dtype=jnp.int32)
    carry, unused = lax.scan(advance, carry, (latent_blocks, rot_blocks, numbers))
    states = carry
    outputs = []
    for state in states:
        best, total, accum = state
        rows = accum.shape[1]
        outputs.append(
            (accum / total[..., None])
            .transpose(1, 0, 2)
            .reshape(rows, local_heads * VDIM)
            .astype(jnp.bfloat16)
        )
    attended = outputs[0]
    return lax.psum_scatter(
        (
            jnp.dot(conv_result, conv_project, preferred_element_type=jnp.float32)
            + jnp.dot(attended, attend_project, preferred_element_type=jnp.float32)
        ).astype(jnp.bfloat16),
        "tp",
        scatter_dimension=0,
        tiled=True,
    )


def solution(mesh):
    in_specs = (
        P("sp", "tp"),
        P(None, "tp"),
        P(None, "tp"),
        P(None, "tp"),
        P(None, "tp"),
        P(None, "tp"),
        P(None, "tp"),
        P(),
        P(),
        P(),
        P(None, "tp"),
        P(None, "tp"),
        P("tp", None),
        P("tp", None),
    )
    out_specs = P(("sp", "tp"), None)
    return jax.shard_map(local, mesh=mesh, in_specs=in_specs, out_specs=out_specs, check_vma=False)
```

profile of v0, /device:TPU:0, one launch (start us, length us, event | category | flops | bytes accessed | tf_op | source)
XLA Modules:
  0.0 229.9 jit_solution(8106722850243884223)
XLA Ops:
  7.3 13.4 %all-gather.3.cloned.1.call-done = bf16[256,2048]{1,0:T(8,128)(2,1)} async-done(((bf16[256,1024]{1,0:T(8,128)(2,1)}), bf16[256,2048]{1,0:T(8,128)(2,1)}) %all-gather.3.cloned.1.call-update) | async-done | bytes 1048592 | tf_op jit(solution)/shard_map/all_gather | solution.py:59
  20.7 1.9 convolution_convert_fusion.2
  22.5 1.9 all_gather.16
  26.2 2.4 %fusion.46 = f32[256,512]{1,0:T(8,128)S(1)} fusion(bf16[256,2048]{1,0:T(8,128)(2,1)S(1)} %copy-done.2, bf16[2048,512]{1,0:T(8,128)(2,1)} %param.22), kind=kOutput, calls=%fused_computation.75 | convolution fusion | flops 536870912 | bytes 3670016 | tf_op jit(solution)/shard_map/dot_general | solution.py:61
  29.4 3.8 %collective-permute-start = (bf16[2,512]{1,0:T(2,128)(2,1)S(1)}, bf16[2,512]{1,0:T(2,128)(2,1)S(1)}, u32[]{:S(2)}, u32[]{:S(2)}) collective-permute-start(bf16[2,512]{1,0:T(2,128)(2,1)S(1)} %slice.66), channel_id=1, source_target_pairs={{0,2},{2,4},{4,6},{6,8},{8,10},{10,12},{12,14},{14,16},{16,18},{18... | collective-permute-start | bytes 6152 | tf_op jit(solution)/shard_map/ppermute | solution.py:18
  33.6 2.0 all_gather.18
  36.2 40.8 %all_gather.19 = bf16[4096,32]{0,1:T(8,128)(2,1)S(1)} all-gather(bf16[256,32]{0,1:T(8,128)(2,1)S(1)} %pad_maximum_fusion.1), channel_id=1, replica_groups=mesh['sp'=16,'tp'=2] {'sp'}, dimensions={0}, use_global_device_ids=true | all-gather | bytes 278528 | tf_op jit(solution)/shard_map/all_gather | solution.py:124
  78.5 0.9 maximum_convert_fusion
  79.4 4.7 %fusion.24 = f32[256,2048]{1,0:T(8,128)} fusion(bf16[512,2048]{1,0:T(8,128)(2,1)S(1)} %copy-done, bf16[256,2048]{1,0:T(8,128)(2,1)S(1)} %copy-done.2, bf16[2048,512]{1,0:T(8,128)(2,1)} %param.21, f32[258,512]{1,0:T(8,128)} %maximum_convert_fusion, f32[512]{0:T(512)S(1)} %bitcast.60, f32[512]{0:T(512)S(1)} %bitcast.59, f32[512]{0:T(512)S(1)} %bitcast.58), kind=kOutput, calls=%fused_computation.32 | convolution fusion | flops 1074659328 | bytes 8919040 | tf_op jit(solution)/shard_map/dot_general | solution.py:171
  84.1 3.9 %all-gather.5.cloned.1.call-done = bf16[4096,256]{1,0:T(8,128)(2,1)} async-done(((bf16[256,256]{1,0:T(8,128)(2,1)}), bf16[4096,256]{1,0:T(8,128)(2,1)}) %all-gather.5.cloned.1.call-update) | async-done | bytes 2097168 | tf_op jit(solution)/shard_map/all_gather | solution.py:123
  88.6 0.8 broadcast_in_dim.24
  89.5 37.1 %while.15 = (s32[]{:T(128)}, f32[8,256]{1,0:T(8,128)S(1)}, f32[8,256]{1,0:T(8,128)S(1)}, f32[8,256,64]{1,2,0:T(8,128)}, s32[8]{0:T(128)}, /*index=5*/s32[]{:T(12...) while((s32[]{:T(128)}, f32[8,256]{1,0:T(8,128)S(1)}, ...), condition=%wide.region_10.11_spmd.clone, body=%wide.region_3.10_spmd.clone.sunk | while | flops 613290752 | bytes 36222520 | solution.py:156
  89.5 1.3 dynamic_slice.39
  92.5 12.1 %conditional.4 = ((f32[8,256]{1,0:T(8,128)S(1)}, f32[8,256]{1,0:T(8,128)S(1)}, f32[8,256,64]{1,2,0:T(8,128)})) conditional(s32[]{:T(128)} %convert_element_type.122, (s32[]{:T(128)}, s32[]{:T(128)}, bf16[8,512,256]{2,1,0:T(8,128)(2,1)}, s32[]{:T(128)}, bf16[256,1024]{1,0:T(8,128)(2,1)}, /*index=5*/s32[]{:T(128)}, bf16[256,8,64]{0,2,1:T(8,128)(2,1)S(1)}, ...), branch_computations={%region_4.8_spmd, %region_9.9_spmd} | conditional | flops 613290752 | bytes 36204816 | solution.py:153
  92.5 1.6 convolution_convert_fusion
  94.1 1.3 broadcast_add_fusion
  96.0 8.7 %conditional = (f32[8,256]{1,0:T(8,128)S(1)}, f32[8,256]{1,0:T(8,128)S(1)}, f32[8,256,64]{1,2,0:T(8,128)}) conditional(s32[]{:T(128)} %convert_element_type.52, (s32[]{:T(128)}, s32[256]{0:T(256)}, bf16[512,1024]{1,0:T(8,128)(2,1)S(1)}, bf16[256,8,64]{0,2,1:T(8,128)(2,1)S(1)}, bf16[8,512,32]{1,2,0:T(8,128)(2,1)}, /*index=5*/s32[]{:T(128)}, ...), branch_computations={%region_5.6_spmd, %region_8.7_spmd} | conditional | flops 344330752 | bytes 34367116 | solution.py:142
  96.0 1.3 copy.22
  97.3 1.8 fusion.13
  99.3 2.0 fusion.44
  101.3 1.1 fusion.5
  102.7 1.2 fusion.9
  104.6 1.3 dynamic_slice.39
  107.8 1.3 dynamic_slice.39
  110.9 1.3 dynamic_slice.39
  114.0 1.3 dynamic_slice.39
  117.2 1.3 dynamic_slice.39
  120.3 1.3 dynamic_slice.39
  123.4 1.3 dynamic_slice.39
  126.5 1.1 divide_convert_fusion
  127.6 3.9 %fusion.21 = bf16[256,2048]{1,0:T(8,128)(2,1)} fusion(f32[256,2048]{1,0:T(8,128)} %fusion.24, bf16[256,512]{0,1:T(8,128)(2,1)S(1)} %bitcast.55, bf16[512,2048]{1,0:T(8,128)(2,1)} %param.33), kind=kOutput, calls=%fused_computation.26 | convolution fusion | flops 537919488 | bytes 5505024 | tf_op jit(solution)/shard_map/dot_general | solution.py:172
  131.6 91.8 %reduce-scatter.2.cloned.1.call-done = bf16[128,2048]{1,0:T(8,128)(2,1)} async-done(((bf16[256,2048]{1,0:T(8,128)(2,1)}), bf16[128,2048]{1,0:T(8,128)(2,1)}) %reduce-scatter.2.cloned.1.call-update) | async-done | bytes 524304 | tf_op jit(solution)/shard_map/reduce_scatter | solution.py:169
  (90 shorter events, 12.2 us)
Async XLA Ops:
  6.5 72.9 %copy-start = (bf16[512,2048]{1,0:T(8,128)(2,1)S(1)}, bf16[512,2048]{1,0:T(8,128)(2,1)}, u32[]{:S(2)}) copy-start(bf16[512,2048]{1,0:T(8,128)(2,1)} %param.32) | copy-start | bytes 6291460
  6.5 18.1 %copy-start.12 = (f32[256]{0:T(256)S(1)}, f32[256]{0:T(256)}, u32[]{:S(2)}) copy-start(f32[256]{0:T(256)} %param.29) | copy-start | bytes 3076
  6.5 19.6 %copy-start.10 = (bf16[3,512]{1,0:T(4,128)(2,1)S(1)}, bf16[3,512]{1,0:T(4,128)(2,1)}, u32[]{:S(2)}) copy-start(bf16[3,512]{1,0:T(4,128)(2,1)} %param.24) | copy-start | bytes 9220
  6.5 14.1 %all-gather.3.cloned.1.call-start = ((), (), s32[]{:S(2)}) async-start(), calls=%async_computation.1 | async-start | bytes 1572864 | tf_op jit(solution)/shard_map/all_gather | solution.py:59
  7.3 80.8 %all-gather.5.cloned.1.call-start = ((), (), s32[]{:S(2)}) async-start(), calls=%async_computation.2 | async-start | bytes 2228224 | tf_op jit(solution)/shard_map/all_gather | solution.py:123
  20.7 5.5 %copy-start.2 = (bf16[256,2048]{1,0:T(8,128)(2,1)S(1)}, bf16[256,2048]{1,0:T(8,128)(2,1)}, u32[]{:S(2)}) copy-start(bf16[256,2048]{1,0:T(8,128)(2,1)} %all-gather.3.cloned.1.call-done) | copy-start | bytes 3145732
  25.4 198.0 %reduce-scatter.2.cloned.1.call-start = ((), (), s32[]{:S(2)}) async-start(), calls=%async_computation.3 | async-start | bytes 1572864 | tf_op jit(solution)/shard_map/reduce_scatter | solution.py:169
  26.1 2.5 %copy-start.5 = (bf16[2048,512]{1,0:T(8,128)(2,1)S(1)}, bf16[2048,512]{1,0:T(8,128)(2,1)}, u32[]{:S(2)}) copy-start(bf16[2048,512]{1,0:T(8,128)(2,1)} %param.23) | copy-start | bytes 6291460
  28.6 4.6 %copy-start.6 = (bf16[2048,256]{1,0:T(8,128)(2,1)S(1)}, bf16[2048,256]{1,0:T(8,128)(2,1)}, u32[]{:S(2)}) copy-start(bf16[2048,256]{1,0:T(8,128)(2,1)} %param.25) | copy-start | bytes 3145732
  29.3 6.3 %copy-start.8 = (bf16[2048,32]{0,1:T(8,128)(2,1)S(1)}, bf16[2048,32]{0,1:T(8,128)(2,1)}, u32[]{:S(2)}) copy-start(bf16[2048,32]{0,1:T(8,128)(2,1)} %param.27) | copy-start | bytes 393220
  29.4 47.8 %copy-start.7 = (bf16[512,768]{1,0:T(8,128)(2,1)S(1)}, bf16[512,768]{1,0:T(8,128)(2,1)}, u32[]{:S(2)}) copy-start(bf16[512,768]{1,0:T(8,128)(2,1)} %param.30) | copy-start | bytes 2359300
  29.4 47.8 %copy-start.11 = (f32[512]{0:T(512)S(1)}, f32[512]{0:T(512)}, u32[]{:S(2)}) copy-start(f32[512]{0:T(512)} %param.28) | copy-start | bytes 6148
  29.4 49.1 %collective-permute-start = (bf16[2,512]{1,0:T(2,128)(2,1)S(1)}, bf16[2,512]{1,0:T(2,128)(2,1)S(1)}, u32[]{:S(2)}, u32[]{:S(2)}) collective-permute-start(bf16[2,512]{1,0:T(2,128)(2,1)S(1)} %slice.66), channel_id=1, source_target_pairs={{0,2},{2,4},{4,6},{6,8},{8,10},{10,12},{12,14},{14,16},{16,18},{18... | collective-permute-start | bytes 6152 | tf_op jit(solution)/shard_map/ppermute | solution.py:18
  97.3 1.8 copy-start.9
  101.3 1.2 copy-start.1
  101.3 1.3 copy-start.3
  103.8 0.8 copy-start.4
Sparse Core Ops, SparseCore 0:
  8.9 11.7 all-gather.2
  25.5 62.4 all-gather.4
  131.7 91.6 reduce-scatter.1
where the time goes:
time: 232 us; the launch traced here: 230 us
  waiting for transfers between devices  110 us (47%)
  blocking collectives  44.7 us (19%)
  matrix products  21.5 us (9%)
  local copies, waits for them, and re-layouts  19.4 us (8%)
  between operations  13.3 us (6%)
  loops' own time  11 us (5%)
  other arithmetic  6.35 us (3%)
  starting transfers between devices  3.85 us (2%)
    reduce_scatter x1, waiting for transfers between devices, local(): lax.psum_scatter((jnp.dot(conv_result, conv_project, preferred_element_ty...  91.8 us
    all_gather x1, blocking collectives, local(): keys_rot = lax.all_gather(rotary_key, 'sp', axis=0, tiled=True)  40.8 us
    all_gather x1, waiting for transfers between devices, local(): piece = lax.all_gather(tokens, 'tp', axis=1, tiled=True)  13.4 us
    dynamic_slice x8, local copies, waits for them, and re-layouts, local(): lax.scan(advance, carry, (latent_blocks, rot_blocks, numbers))  10.2 us
    another operation x1, loops' own time, local(): lax.scan(advance, carry, (latent_blocks, rot_blocks, numbers))  10 us
    dot_general x5, matrix products, local(): jnp.dot(piece, weight, preferred_element_type=jnp.float32)  5.85 us
    dot_general x1, matrix products, local(): jnp.dot(conv_result, conv_project, preferred_element_type=jnp.float32)  4.74 us
  transfers between devices with their start and end apart: 4, of which 3 were waited for; matrix products, arithmetic and copies ran while one was open for 5% of the time, Pallas kernels for 0%

commit v1 on v0

--- a/solution.py
+++ b/solution.py
@@ -120,8 +120,13 @@
         )
     )
     carry = initial
-    keys_latent = lax.all_gather(latent_norm, "sp", axis=0, tiled=True)
-    keys_rot = lax.all_gather(rotary_key, "sp", axis=0, tiled=True)
+    keys_latent, keys_rot = jnp.split(
+        lax.all_gather(
+            jnp.concatenate([latent_norm, rotary_key], axis=1), "sp", axis=0, tiled=True
+        ),
+        [latent_norm.shape[1]],
+        axis=1,
+    )
     count = keys_latent.shape[0]
     block = math.gcd(count, 512)
     latent_blocks = keys_latent.reshape(count // block, block, keys_latent.shape[1])

time: 232 us -> 246 us (1.060)
  waiting for transfers between devices: 110 us -> 158 us
  blocking collectives: 44.7 us -> 3.92 us
  local copies, waits for them, and re-layouts: 19.4 us -> 23.8 us
    all_gather x1, waiting for transfers between devices: 3.88 us -> 52.6 us  [local(): lax.all_gather(jnp.concatenate([latent_norm, rotary_key], axis=1), 'sp',...]
    all_gather x1 -> x0, blocking collectives: 40.8 us -> none  [local(): keys_rot = lax.all_gather(rotary_key, 'sp', axis=0, tiled=True)]
    split x0 -> x3, local copies, waits for them, and re-layouts: none -> 4.3 us  [local(): jnp.split(lax.all_gather(jnp.concatenate([latent_norm, rotary_key], axis=...]
  transfers between devices with their start and end apart: 4 -> 4, of which waited for: 3 -> 3; matrix products, arithmetic and copies ran while one was open for 5% -> 4% of each run, Pallas kernels for 0% -> 0%
where the time goes in v1:
time: 246 us; the launch traced here: 244 us
  waiting for transfers between devices  158 us (64%)
  local copies, waits for them, and re-layouts  23.8 us (10%)
  matrix products  22.8 us (9%)
  between operations  13.4 us (5%)
  loops' own time  11.4 us (5%)
  other arithmetic  6.47 us (3%)
  blocking collectives  3.92 us (2%)
  starting transfers between devices  3.85 us (2%)
    reduce_scatter x1, waiting for transfers between devices, local(): lax.psum_scatter((jnp.dot(conv_result, conv_project, preferred_element_ty...  91.4 us
    all_gather x1, waiting for transfers between devices, local(): lax.all_gather(jnp.concatenate([latent_norm, rotary_key], axis=1), 'sp',...  52.6 us
    all_gather x1, waiting for transfers between devices, local(): piece = lax.all_gather(tokens, 'tp', axis=1, tiled=True)  13.3 us
    another operation x1, loops' own time, local(): lax.scan(advance, carry, (latent_blocks, rot_blocks, numbers))  10.5 us
    dynamic_slice x8, local copies, waits for them, and re-layouts, local(): lax.scan(advance, carry, (latent_blocks, rot_blocks, numbers))  9.8 us
    dot_general x5, matrix products, local(): jnp.dot(piece, weight, preferred_element_type=jnp.float32)  7.08 us
  transfers between devices with their start and end apart: 4, of which 3 were waited for; matrix products, arithmetic and copies ran while one was open for 4% of the time, Pallas kernels for 0%

profile of v1, /device:TPU:0, one launch (start us, length us, event | category | flops | bytes accessed | tf_op | source)
XLA Modules:
  0.0 243.7 jit_solution(11248025624507622457)
XLA Ops:
  7.4 13.3 %all-gather.3.cloned.1.call-done = bf16[256,2048]{1,0:T(8,128)(2,1)} async-done(((bf16[256,1024]{1,0:T(8,128)(2,1)}), bf16[256,2048]{1,0:T(8,128)(2,1)}) %all-gather.3.cloned.1.call-update) | async-done | bytes 1048592 | tf_op jit(solution)/shard_map/all_gather | solution.py:59
  20.7 1.9 convolution_convert_fusion.2
  22.5 1.9 all_gather.13
  24.6 1.6 fusion.47
  28.3 2.4 fusion.46
  31.5 3.8 %collective-permute-start = (bf16[2,512]{1,0:T(2,128)(2,1)S(1)}, bf16[2,512]{1,0:T(2,128)(2,1)S(1)}, u32[]{:S(2)}, u32[]{:S(2)}) collective-permute-start(bf16[2,512]{1,0:T(2,128)(2,1)S(1)} %slice.66), channel_id=1, source_target_pairs={{0,2},{2,4},{4,6},{6,8},{8,10},{10,12},{12,14},{14,16},{16,18},{18... | collective-permute-start | bytes 6152 | tf_op jit(solution)/shard_map/ppermute | solution.py:18
  35.7 2.0 all_gather.15
  39.4 4.8 %fusion.24 = f32[256,2048]{1,0:T(8,128)} fusion(bf16[512,2048]{1,0:T(8,128)(2,1)S(1)} %copy-done, bf16[256,2048]{1,0:T(8,128)(2,1)S(1)} %copy-done.2, bf16[2048,512]{1,0:T(8,128)(2,1)} %param.21, f32[258,512]{1,0:T(8,128)} %maximum_convert_fusion, f32[512]{0:T(512)S(1)} %bitcast.56, f32[512]{0:T(512)S(1)} %bitcast.55, f32[512]{0:T(512)S(1)} %bitcast.54), kind=kOutput, calls=%fused_computation.32 | convolution fusion | flops 1074659328 | bytes 8919040 | tf_op jit(solution)/shard_map/dot_general | solution.py:176
  44.2 52.6 %all-gather.5.cloned.1.call-done = bf16[4096,288]{1,0:T(8,128)(2,1)} async-done(((bf16[256,288]{1,0:T(8,128)(2,1)}), bf16[4096,288]{1,0:T(8,128)(2,1)}) %all-gather.5.cloned.1.call-update) | async-done | bytes 2359312 | tf_op jit(solution)/shard_map/all_gather | solution.py:124
  96.8 1.2 slice-done
  99.0 3.1 %split.8 = bf16[4096,256]{1,0:T(8,128)(2,1)} slice(bf16[4096,288]{1,0:T(8,128)(2,1)} %all-gather.5.cloned.1.call-done), slice={[0:4096], [0:256]} | slice | bytes 4194304 | tf_op jit(solution)/shard_map/split | solution.py:123
  103.4 37.2 %while.15 = (s32[]{:T(128)}, f32[8,256]{1,0:T(8,128)S(1)}, f32[8,256]{1,0:T(8,128)S(1)}, f32[8,256,64]{1,2,0:T(8,128)}, s32[8]{0:T(128)}, /*index=5*/s32[]{:T(12...) while((s32[]{:T(128)}, f32[8,256]{1,0:T(8,128)S(1)}, ...), condition=%wide.region_10.11_spmd.clone, body=%wide.region_3.10_spmd.clone.sunk | while | flops 613290752 | bytes 36222520 | solution.py:161
  103.4 1.2 dynamic_slice.39
  106.5 12.1 %conditional.4 = ((f32[8,256]{1,0:T(8,128)S(1)}, f32[8,256]{1,0:T(8,128)S(1)}, f32[8,256,64]{1,2,0:T(8,128)})) conditional(s32[]{:T(128)} %convert_element_type.122, (s32[]{:T(128)}, s32[]{:T(128)}, bf16[8,512,256]{2,1,0:T(8,128)(2,1)}, s32[]{:T(128)}, bf16[256,1024]{1,0:T(8,128)(2,1)}, /*index=5*/s32[]{:T(128)}, bf16[256,8,64]{0,2,1:T(8,128)(2,1)S(1)}, ...), branch_computations={%region_4.8_spmd, %region_9.9_spmd} | conditional | flops 613290752 | bytes 36204816 | solution.py:158
  106.5 1.6 convolution_convert_fusion
  108.1 1.2 broadcast_add_fusion
  110.0 8.6 %conditional = (f32[8,256]{1,0:T(8,128)S(1)}, f32[8,256]{1,0:T(8,128)S(1)}, f32[8,256,64]{1,2,0:T(8,128)}) conditional(s32[]{:T(128)} %convert_element_type.52, (s32[]{:T(128)}, s32[256]{0:T(256)}, bf16[512,1024]{1,0:T(8,128)(2,1)S(1)}, bf16[256,8,64]{0,2,1:T(8,128)(2,1)S(1)}, bf16[8,512,32]{1,2,0:T(8,128)(2,1)}, /*index=5*/s32[]{:T(128)}, ...), branch_computations={%region_5.6_spmd, %region_8.7_spmd} | conditional | flops 344330752 | bytes 34367116 | solution.py:147
  110.0 1.3 copy.34
  111.3 1.8 fusion.13
  113.3 2.0 fusion.44
  115.3 1.1 fusion.5
  116.6 1.2 fusion.9
  118.6 1.2 dynamic_slice.39
  121.8 1.2 dynamic_slice.39
  124.9 1.2 dynamic_slice.39
  128.1 1.2 dynamic_slice.39
  131.2 1.2 dynamic_slice.39
  134.4 1.2 dynamic_slice.39
  137.5 1.2 dynamic_slice.39
  140.7 1.1 divide_convert_fusion
  141.8 3.9 %fusion.21 = bf16[256,2048]{1,0:T(8,128)(2,1)} fusion(f32[256,2048]{1,0:T(8,128)} %fusion.24, bf16[256,512]{0,1:T(8,128)(2,1)S(1)} %bitcast.53, bf16[512,2048]{1,0:T(8,128)(2,1)} %param.33), kind=kOutput, calls=%fused_computation.26 | convolution fusion | flops 537919488 | bytes 5505024 | tf_op jit(solution)/shard_map/dot_general | solution.py:177
  145.7 91.4 %reduce-scatter.2.cloned.1.call-done = bf16[128,2048]{1,0:T(8,128)(2,1)} async-done(((bf16[256,2048]{1,0:T(8,128)(2,1)}), bf16[128,2048]{1,0:T(8,128)(2,1)}) %reduce-scatter.2.cloned.1.call-update) | async-done | bytes 524304 | tf_op jit(solution)/shard_map/reduce_scatter | solution.py:174
  (94 shorter events, 14.1 us)
Async XLA Ops:
  6.5 32.9 %copy-start = (bf16[512,2048]{1,0:T(8,128)(2,1)S(1)}, bf16[512,2048]{1,0:T(8,128)(2,1)}, u32[]{:S(2)}) copy-start(bf16[512,2048]{1,0:T(8,128)(2,1)} %param.32) | copy-start | bytes 6291460
  6.5 18.1 %copy-start.8 = (bf16[2048,32]{0,1:T(8,128)(2,1)S(1)}, bf16[2048,32]{0,1:T(8,128)(2,1)}, u32[]{:S(2)}) copy-start(bf16[2048,32]{0,1:T(8,128)(2,1)} %param.27) | copy-start | bytes 393220
  6.5 20.1 %copy-start.12 = (f32[256]{0:T(256)S(1)}, f32[256]{0:T(256)}, u32[]{:S(2)}) copy-start(f32[256]{0:T(256)} %param.29) | copy-start | bytes 3076
  6.5 14.1 %all-gather.3.cloned.1.call-start = ((), (), s32[]{:S(2)}) async-start(), calls=%async_computation.1 | async-start | bytes 1572864 | tf_op jit(solution)/shard_map/all_gather | solution.py:59
  7.3 89.5 %all-gather.5.cloned.1.call-start = ((), (), s32[]{:S(2)}) async-start(), calls=%async_computation.2 | async-start | bytes 3342336 | tf_op jit(solution)/shard_map/all_gather | solution.py:124
  7.3 20.9 %copy-start.10 = (bf16[3,512]{1,0:T(4,128)(2,1)S(1)}, bf16[3,512]{1,0:T(4,128)(2,1)}, u32[]{:S(2)}) copy-start(bf16[3,512]{1,0:T(4,128)(2,1)} %param.24) | copy-start | bytes 9220
  20.7 7.6 %copy-start.2 = (bf16[256,2048]{1,0:T(8,128)(2,1)S(1)}, bf16[256,2048]{1,0:T(8,128)(2,1)}, u32[]{:S(2)}) copy-start(bf16[256,2048]{1,0:T(8,128)(2,1)} %all-gather.3.cloned.1.call-done) | copy-start | bytes 3145732
  27.6 209.6 %reduce-scatter.2.cloned.1.call-start = ((), (), s32[]{:S(2)}) async-start(), calls=%async_computation.3 | async-start | bytes 1572864 | tf_op jit(solution)/shard_map/reduce_scatter | solution.py:174
  28.3 2.5 %copy-start.5 = (bf16[2048,512]{1,0:T(8,128)(2,1)S(1)}, bf16[2048,512]{1,0:T(8,128)(2,1)}, u32[]{:S(2)}) copy-start(bf16[2048,512]{1,0:T(8,128)(2,1)} %param.23) | copy-start | bytes 6291460
  30.8 4.5 %copy-start.6 = (bf16[2048,256]{1,0:T(8,128)(2,1)S(1)}, bf16[2048,256]{1,0:T(8,128)(2,1)}, u32[]{:S(2)}) copy-start(bf16[2048,256]{1,0:T(8,128)(2,1)} %param.25) | copy-start | bytes 3145732
  31.5 6.4 %copy-start.7 = (bf16[512,768]{1,0:T(8,128)(2,1)S(1)}, bf16[512,768]{1,0:T(8,128)(2,1)}, u32[]{:S(2)}) copy-start(bf16[512,768]{1,0:T(8,128)(2,1)} %param.30) | copy-start | bytes 2359300
  31.5 6.4 %copy-start.11 = (f32[512]{0:T(512)S(1)}, f32[512]{0:T(512)}, u32[]{:S(2)}) copy-start(f32[512]{0:T(512)} %param.28) | copy-start | bytes 6148
  31.5 7.0 %collective-permute-start = (bf16[2,512]{1,0:T(2,128)(2,1)S(1)}, bf16[2,512]{1,0:T(2,128)(2,1)S(1)}, u32[]{:S(2)}, u32[]{:S(2)}) collective-permute-start(bf16[2,512]{1,0:T(2,128)(2,1)S(1)} %slice.66), channel_id=1, source_target_pairs={{0,2},{2,4},{4,6},{6,8},{8,10},{10,12},{12,14},{14,16},{16,18},{18... | collective-permute-start | bytes 6152 | tf_op jit(solution)/shard_map/ppermute | solution.py:18
  96.8 1.2 slice-start
  111.3 1.8 copy-start.9
  115.3 1.2 copy-start.1
  115.3 1.3 copy-start.3
  117.8 0.8 copy-start.4
Sparse Core Ops, SparseCore 0:
  8.9 11.7 all-gather.2
  27.7 69.0 all-gather.4
  145.8 91.2 reduce-scatter.1
